TPU v7x, 32 devices: a whole 2x2x4 slice. The times are simulated.
32 devices in a mesh: sp: 8 (over z, x), tp: 4 (over y, core).
Axes of the slice: x: 2, y: 2, z: 4, core: 2. Of those that a mesh axis runs over, the one named last changes fastest.
Arguments:
- moe_in: bfloat16 [1536, 2048], P('sp', 'tp'), may hold values from -6 to 6
- cotangent: bfloat16 [1536, 2048], P('sp', 'tp'), may hold values from -6 to 6
- routes: int32 [1536, 2], P('sp'), may hold values from 0 to 7, all different within a row; in each aligned block of 192 rows (0 to 191, 192 to 383, ...) at most 60 rows name the same one
- route_weight: float32 [1536, 2], P('sp'), may hold values from 0.2 to 1
- w_gate: bfloat16 [8, 3584, 2048], P('sp', 'tp'), may hold values from -0.125 to 0.125
- w_up: bfloat16 [8, 3584, 2048], P('sp', 'tp'), may hold values from -0.125 to 0.125
- w_down: bfloat16 [8, 3584, 2048], P('sp', 'tp'), may hold values from -0.09375 to 0.09375
- conv_pre: bfloat16 [1536, 2048], P('sp', 'tp'), may hold values from -6 to 6
- norm_mean: float32 [1536], P('sp'), may hold values from -3 to 3
- norm_rstd: float32 [1536], P('sp'), may hold values from 0.5 to 2
- ln_gain: float32 [2048], P('tp'), may hold values from 0.1 to 1.9
- ln_shift: float32 [2048], P('tp'), may hold values from -3 to 3
- taps: float32 [31, 2048], P(None, 'tp'), may hold values from -1 to 1
- w_proj: bfloat16 [2048, 2048], P('sp', 'tp'), may hold values from -0.125 to 0.125
Outputs:
- grad_up: bfloat16 [8, 3584, 2048], P('sp', 'tp')
- grad_down: bfloat16 [8, 3584, 2048], P('sp', 'tp')
- grad_stream: bfloat16 [1536, 2048], P('sp', 'tp')
- grad_proj: float32 [2048, 2048], P('sp', 'tp')
- grad_conv: bfloat16 [1536, 2048], P('sp', 'tp')
Inputs may be any that keep to these rules, and one draw needn't show every extreme that they name: `routes`: each token names 2 different experts. Among the tokens of one index of sp no expert is named more than 60 times, a bound that some block reaches.
All inputs are finite; a program needn't handle non-finite values.
Results may differ from a plain program's by a relative error of at most 0.02.
Values may be sent and summed in bfloat16 or wider, within the bound.
A program may use at most 64 MiB of HBM per device.

v0:
```python
import functools

import jax
import jax.numpy as jnp
from jax import lax
from jax.experimental import pallas as pl
from jax.experimental.pallas import tpu as pltpu
from jax.sharding import PartitionSpec as P

MESH = pl.DeviceIdType.MESH
BF = jnp.bfloat16
F32 = jnp.float32


def flipped(index, step):
    value, bit = index, 1
    while bit <= step:
        if step & bit:
            value = value + bit * (1 - 2 * lax.rem(lax.div(index, bit), 2))
        bit *= 2
    return value


def tile(index, size):
    return pl.ds(pl.multiple_of(index * size, size), size)


def nn(left, right):
    return lax.dot_general(left, right, (((1,), (0,)), ((), ())), preferred_element_type=F32)


def nt(left, right):
    return lax.dot_general(left, right, (((1,), (1,)), ((), ())), preferred_element_type=F32)


def tn(left, right):
    return lax.dot_general(left, right, (((0,), (0,)), ((), ())), preferred_element_type=F32)


def layer_kernel(
    groups, lanes, across,
    moe_ref, cot_ref, cols_ref, lines_ref, conv_ref, gain_ref, shift_ref, taps_ref,
    gate_hbm, up_hbm, down_hbm, proj_hbm,
    gup_ref, gdown_ref, gstream_ref, gproj_ref, gconv_ref,
    gate_w, up_w, down_w, send, rows, work_a, work_b, work_c, hid, upg, gtg,
    part, half, summed, arrived, total, returned, chosen_back, gathered, mix, pieces,
    normed_s, slope_s, stat_out, stat_in, ext,
    load_sem, dsp_s, dsp_r, dy_s, dy_r, dc_s, dc_r, sw_s, sw_r, cy_s, cy_r, csp_s, csp_r,
    az_s, az_r, ax_s, ax_r, ty_s, ty_r, tc_s, tc_r, p_s, p_r, st_s, st_r, halo_s, halo_r,
):
    group, lane = (lax.axis_index("sp"), lax.axis_index("tp"))
    chips = lanes // 2
    depth = groups // across
    chip, core = (lax.div(lane, 2), lax.rem(lane, 2))
    level, column = (lax.div(group, across), lax.rem(group, across))
    tokens, width = moe_ref.shape
    channels = width * lanes
    hidden_units = gate_w.shape[0]
    slots = groups * (rows.shape[1] // groups)
    cap = slots // groups
    halves = 2
    per_half = groups // halves
    half_rows = slots // halves
    proj_rows = proj_hbm.shape[0]
    lag_count = taps_ref.shape[0]
    partner = (group, flipped(lane, 1))
    mine = tile(lane, width)

    barrier = pltpu.get_barrier_semaphore()
    for step in range(1, groups):
        pl.semaphore_signal(barrier, inc=1, device_id=(flipped(group, step), lane), device_id_type=MESH)
    for step in range(1, lanes):
        pl.semaphore_signal(barrier, inc=1, device_id=(group, flipped(lane, step)), device_id_type=MESH)

    def remote(source, target, sends, recvs, device):
        return pltpu.make_async_remote_copy(
            src_ref=source, dst_ref=target, send_sem=sends, recv_sem=recvs,
            device_id=device, device_id_type=MESH,
        )

    loads = [
        pltpu.make_async_copy(proj_hbm, gathered.at[group, pl.ds(0, proj_rows)], load_sem.at[0]),
        pltpu.make_async_copy(gate_hbm.at[0], gate_w, load_sem.at[1]),
        pltpu.make_async_copy(up_hbm.at[0], up_w, load_sem.at[2]),
        pltpu.make_async_copy(down_hbm.at[0], down_w, load_sem.at[3]),
    ]
    for copy in loads:
        copy.start()

    named_line = (lines_ref[0:1, :], lines_ref[1:2, :])
    weight_line = (lines_ref[2:3, :], lines_ref[3:4, :])
    named_col = (cols_ref[:, 2:3], cols_ref[:, 3:4])
    down_iota = lax.broadcasted_iota(jnp.int32, (tokens, tokens), 0)
    over_iota = lax.broadcasted_iota(jnp.int32, (tokens, tokens), 1)
    place = lax.broadcasted_iota(jnp.int32, (slots, tokens), 0).astype(F32)
    matches, slot_weight = ([], 0.0)
    for choice in range(2):
        same = jnp.where(named_col[0] == named_line[choice], 1.0, 0.0) + jnp.where(
            named_col[1] == named_line[choice], 1.0, 0.0
        )
        rank = jnp.sum(jnp.where(down_iota < over_iota, same, 0.0), axis=0, keepdims=True)
        match = place == named_line[choice] * float(cap) + rank
        matches.append(match)
        slot_weight = slot_weight + jnp.sum(
            jnp.where(match, weight_line[choice], 0.0), axis=1, keepdims=True
        )
    chosen = jnp.where(matches[0] | matches[1], 1.0, 0.0).astype(BF)
    send[0] = nn(chosen, moe_ref[...]).astype(BF)
    send[1] = (slot_weight * nn(chosen, cot_ref[...])).astype(BF)
    rows[0, 0:cap, mine] = send[0, 0:cap, :]
    rows[1, 0:cap, mine] = send[1, 0:cap, :]

    pl.semaphore_wait(barrier, groups + lanes - 2)

    def at_slot(step, lane_index):
        return rows.at[:, pl.ds(step * cap, cap), tile(lane_index, width)]

    outgoing = []

    def go(copy):
        copy.start()
        outgoing.append(copy)
        return copy

    dispatched, crossed, shared = ({}, {}, {})

    def forward(step):
        for turn in range(1, chips):
            crossed[step, turn] = go(remote(
                at_slot(step, lane), at_slot(step, lane), dy_s.at[step, turn], dy_r.at[step, turn],
                (group, flipped(lane, 2 * turn)),
            ))
        shared[step, 0] = go(remote(
            at_slot(step, lane), at_slot(step, lane), dc_s.at[step, 0], dc_r.at[step, 0], partner
        ))

    def relay(step):
        for turn in range(1, chips):
            crossed[step, turn].wait_recv()
            peer = flipped(lane, 2 * turn)
            shared[step, turn] = go(remote(
                at_slot(step, peer), at_slot(step, peer), dc_s.at[step, turn], dc_r.at[step, turn], partner
            ))

    forward(0)
    for step in range(1, groups):
        dispatched[step] = go(remote(
            send.at[:, pl.ds(step * cap, cap)], at_slot(step, lane),
            dsp_s.at[step], dsp_r.at[step], (flipped(group, step), lane),
        ))

    bounds = ((0, proj_rows), (proj_rows, tokens))

    def block(owner_level, owner_column, kind):
        return gathered.at[owner_level * across + owner_column, pl.ds(bounds[kind][0], bounds[kind][1])]

    def along(kind, way, hop):
        sign = 1 - 2 * way
        source_level = level - sign * hop
        here = block(source_level, column, kind)
        return remote(
            here, here, az_s.at[kind, way, hop], az_r.at[kind, way, hop],
            ((level + sign) * across + column, lane),
        )

    def along_valid(way, hop):
        if way == 0:
            return (level - hop >= 0) & (level + 1 < depth)
        return (level + hop < depth) & (level - 1 >= 0)

    def arrives_valid(way, hop):
        if way == 0:
            return level - 1 - hop >= 0
        return level + 1 + hop < depth

    def sideways(kind, event, owner_level):
        copies = []
        for turn in range(1, across):
            here = block(owner_level, column, kind)
            copies.append(remote(
                here, here, ax_s.at[kind, event, turn], ax_r.at[kind, event, turn],
                (level * across + flipped(column, turn), lane),
            ))
        return copies

    def gather_own(kind):
        for way in range(2):
            @pl.when(along_valid(way, 0))
            def _():
                along(kind, way, 0).start()
        for copy in sideways(kind, 0, level):
            copy.start()

    def gather_hop(kind, hop):
        for way in range(2):
            sign = 1 - 2 * way

            @pl.when(arrives_valid(way, hop))
            def _():
                along(kind, way, hop).wait_recv()
                if hop + 1 < depth - 1:
                    @pl.when(along_valid(way, hop + 1))
                    def _():
                        along(kind, way, hop + 1).start()
                for copy in sideways(kind, 1 + 2 * hop + way, level - sign * (hop + 1)):
                    copy.start()

    def gather_rest(kind):
        for copy in sideways(kind, 0, level):
            copy.wait()
        for hop in range(depth - 1):
            for way in range(2):
                sign = 1 - 2 * way

                @pl.when(along_valid(way, hop))
                def _():
                    along(kind, way, hop).wait_send()

                @pl.when(arrives_valid(way, hop))
                def _():
                    for copy in sideways(kind, 1 + 2 * hop + way, level - sign * (hop + 1)):
                        copy.wait()

    loads[0].wait()
    gather_own(0)

    normed = (conv_ref[...].astype(F32) - cols_ref[:, 0:1]) * cols_ref[:, 1:2]
    pre_act = normed * gain_ref[...] + shift_ref[...]
    act_sigmoid = jax.nn.sigmoid(pre_act)
    gathered[group, proj_rows : proj_rows + tokens, :] = (pre_act * act_sigmoid).astype(BF)
    normed_s[...] = normed
    slope_s[...] = act_sigmoid * (1.0 + pre_act * (1.0 - act_sigmoid)) * gain_ref[...]
    back_place = lax.broadcasted_iota(jnp.int32, (tokens, slots), 1).astype(F32)
    back = None
    for choice in range(2):
        same = jnp.where(named_line[0] == named_col[choice], 1.0, 0.0) + jnp.where(
            named_line[1] == named_col[choice], 1.0, 0.0
        )
        rank = jnp.sum(jnp.where(over_iota < down_iota, same, 0.0), axis=1, keepdims=True)
        match = back_place == named_col[choice] * float(cap) + rank
        back = match if back is None else back | match
    chosen_back[...] = jnp.where(back, 1.0, 0.0).astype(BF)

    def of_half(part_index):
        return slice(part_index * half_rows, (part_index + 1) * half_rows)

    def activate(part_index):
        here = of_half(part_index)
        step_rows = 64

        def body(index, carry):
            there = tile(index, step_rows)
            gate_pre, up_pre, hidden_grad = (work_a[there, :], work_b[there, :], work_c[there, :])
            gate_sigmoid = jax.nn.sigmoid(gate_pre)
            gate_active = gate_pre * gate_sigmoid
            hid[there, here] = (gate_active * up_pre).astype(BF)
            upg[there, here] = (hidden_grad * gate_active).astype(BF)
            gtg[there, here] = (
                hidden_grad * up_pre * (gate_sigmoid * (1.0 + gate_pre * (1.0 - gate_sigmoid)))
            ).astype(BF)
            return carry

        lax.fori_loop(0, hidden_units // step_rows, body, 0)

    def partial_columns(part_index, lane_index):
        here = of_half(part_index)
        there = tile(lane_index, width)
        value = tn(gtg[:, here], gate_w[:, there]) + tn(upg[:, here], up_w[:, there])
        part[here, there] = value.astype(BF)

    swaps, homeward, back_across = ({}, {}, {})

    def swap(part_index, turn):
        away = flipped(lane, 2 * turn + 1)
        here = pl.ds(part_index * half_rows, half_rows)
        swaps[part_index, turn] = go(remote(
            part.at[here, tile(away, width)], half.at[turn, here],
            sw_s.at[part_index, turn], sw_r.at[part_index, turn], partner,
        ))

    def partials(part_index):
        for turn in [*range(1, chips), 0]:
            partial_columns(part_index, flipped(lane, 2 * turn + 1))
            swap(part_index, turn)
            partial_columns(part_index, flipped(lane, 2 * turn))

    def chip_sums(part_index):
        for turn in range(1, chips):
            away = flipped(lane, 2 * turn)
            swaps[part_index, turn].wait_recv()
            for step in range(part_index * per_half, (part_index + 1) * per_half):
                here = slice(step * cap, (step + 1) * cap)
                summed[turn - 1, here, :] = (
                    part[here, tile(away, width)].astype(F32) + half[turn, here, :].astype(F32)
                ).astype(BF)
                back_across[step, turn] = go(remote(
                    summed.at[turn - 1, pl.ds(step * cap, cap)], arrived.at[turn - 1, pl.ds(step * cap, cap)],
                    cy_s.at[step, turn], cy_r.at[step, turn], (group, away),
                ))

    def send_home(part_index):
        swaps[part_index, 0].wait_recv()
        for step in range(part_index * per_half, (part_index + 1) * per_half):
            here = slice(step * cap, (step + 1) * cap)
            value = part[here, mine].astype(F32) + half[0, here, :].astype(F32)
            for turn in range(1, chips):
                back_across[step, turn].wait_recv()
                value = value + arrived[turn - 1, here, :].astype(F32)
            if step:
                total[here, :] = value.astype(BF)
                homeward[step] = go(remote(
                    total.at[pl.ds(step * cap, cap)], returned.at[pl.ds(step * cap, cap)],
                    csp_s.at[step], csp_r.at[step], (flipped(group, step), lane),
                ))
            else:
                returned[here, :] = value.astype(BF)

    for step in range(1, per_half):
        dispatched[step].wait_recv()
        forward(step)
        relay(step - 1)
    far = list(range(per_half, groups))
    quarter = max(1, len(far) // 4)
    for step in far[:quarter]:
        dispatched[step].wait_recv()
        forward(step)
    relay(per_half - 1)
    for step in range(per_half):
        for turn in range(chips):
            shared[step, turn].wait_recv()
    near = of_half(0)
    for copy in loads[1:]:
        copy.wait()
    work_a[...] = nt(gate_w[...], rows[0, near, :])
    for step in far[quarter : 2 * quarter]:
        dispatched[step].wait_recv()
        forward(step)
    work_b[...] = nt(up_w[...], rows[0, near, :])
    work_c[...] = nt(down_w[...], rows[1, near, :])
    for step in far[2 * quarter : 3 * quarter]:
        dispatched[step].wait_recv()
        forward(step)
    activate(0)
    for step in far[:quarter]:
        relay(step)
    partials(0)
    for step in far[3 * quarter :]:
        dispatched[step].wait_recv()
        forward(step)
    for step in far[quarter:]:
        relay(step)
    chip_sums(0)

    for step in far:
        for turn in range(chips):
            shared[step, turn].wait_recv()
    beyond = of_half(1)
    work_a[...] = nt(gate_w[...], rows[0, beyond, :])
    gather_hop(0, 0)
    work_b[...] = nt(up_w[...], rows[0, beyond, :])
    work_c[...] = nt(down_w[...], rows[1, beyond, :])
    activate(1)
    send_home(0)
    partials(1)
    chip_sums(1)
    for hop in range(1, depth - 1):
        gather_hop(0, hop)
    send_home(1)
    gather_own(1)

    span = min(channels, 512)

    def down_tile(index, carry):
        there = tile(index, span)
        gdown_ref[0, :, there] = nn(hid[...], rows[1, :, there]).astype(BF)
        return carry

    def up_tile(index, carry):
        there = tile(index, span)
        gup_ref[0, :, there] = nn(upg[...], rows[0, :, there]).astype(BF)
        return carry

    lax.fori_loop(0, channels // span, down_tile, 0)
    gather_hop(1, 0)
    lax.fori_loop(0, channels // span, up_tile, 0)

    for step in range(1, groups):
        homeward[step].wait_recv()
    picked = nn(chosen_back[...], returned[...])
    own_stream = (cot_ref[...].astype(F32) + picked).astype(BF)
    gstream_ref[...] = own_stream
    mix[:, mine] = own_stream
    tp_across = {}
    for turn in range(1, chips):
        tp_across[turn] = go(remote(
            mix.at[:, mine], mix.at[:, mine], ty_s.at[turn], ty_r.at[turn], (group, flipped(lane, 2 * turn))
        ))
    tp_shared = {0: go(remote(mix.at[:, mine], mix.at[:, mine], tc_s.at[0], tc_r.at[0], partner))}
    for turn in range(1, chips):
        tp_across[turn].wait_recv()
        theirs = tile(flipped(lane, 2 * turn), width)
        tp_shared[turn] = go(remote(
            mix.at[:, theirs], mix.at[:, theirs], tc_s.at[turn], tc_r.at[turn], partner
        ))
    gather_rest(0)
    for turn in range(chips):
        tp_shared[turn].wait_recv()
    for hop in range(1, depth - 1):
        gather_hop(1, hop)

    share = channels // groups
    piece_width = pieces.shape[2]

    def piece_of(owner):
        if share == piece_width:
            return tile(owner, share)
        return tile(lax.div(owner * share, piece_width), piece_width)

    travelling = {}
    for step in range(1, groups):
        owner = flipped(group, step)
        travelling[step] = go(remote(
            mix.at[:, piece_of(owner)], pieces.at[step], p_s.at[step], p_r.at[step], (owner, lane)
        ))

    whole_proj = gathered[:, 0:proj_rows, :].reshape(groups * proj_rows, width)
    normed_grad = nn(mix[...], whole_proj) * slope_s[...]
    weighted = normed_grad * normed_s[...]
    ones = jnp.ones((16, width), BF)

    def line_sum(value):
        high = value.astype(BF)
        low = (value - high.astype(F32)).astype(BF)
        return nt(ones, high) + nt(ones, low)

    line = lax.broadcasted_iota(jnp.int32, (16, tokens), 0)
    own_stat = jnp.where(line == 0, line_sum(normed_grad), line_sum(weighted))
    stat_out[...] = own_stat
    stats = []
    for step in range(1, lanes):
        stats.append(go(remote(
            stat_out, stat_in.at[step], st_s.at[step], st_r.at[step], (group, flipped(lane, step))
        )))
    all_stat = own_stat
    for step in range(1, lanes):
        stats[step - 1].wait_recv()
        all_stat = all_stat + stat_in[step]
    all_stat = all_stat * (1.0 / channels)
    high = all_stat.astype(BF)
    middle = (all_stat - high.astype(F32)).astype(BF)
    low = (all_stat - high.astype(F32) - middle.astype(F32)).astype(BF)
    pick = lax.broadcasted_iota(jnp.int32, (16, width), 0)

    def spread_line(number):
        chooser = jnp.where(pick == number, 1.0, 0.0).astype(BF)
        return tn(high, chooser) + tn(middle, chooser) + tn(low, chooser)

    ext[0:tokens, :] = cols_ref[:, 1:2] * (
        normed_grad - spread_line(0) - normed_s[...] * spread_line(1)
    )
    rim = ext.shape[0] - tokens

    def halo():
        return remote(
            ext.at[pl.ds(0, rim)], ext.at[pl.ds(tokens, rim)], halo_s, halo_r, (group - 1, lane)
        )

    @pl.when(group > 0)
    def _():
        halo().start()

    def piece_value(value):
        if share == piece_width:
            return value
        per = piece_width // share
        which = lax.rem(group, per)
        result = value[:, 0:share]
        for index in range(1, per):
            result = jnp.where(which == index, value[:, index * share : (index + 1) * share], result)
        return result

    for hop in range(depth - 1, depth - 1):
        gather_hop(1, hop)
    gather_rest(1)
    gproj = tn(piece_value(mix[:, piece_of(group)]), gathered[group, proj_rows : proj_rows + tokens, :])
    for step in range(1, groups):
        travelling[step].wait_recv()
        owner = flipped(group, step)
        gproj = gproj + tn(piece_value(pieces[step]), gathered[owner, proj_rows : proj_rows + tokens, :])
    gproj_ref[...] = gproj

    @pl.when(group < groups - 1)
    def _():
        halo().wait_recv()

    @pl.when(group == groups - 1)
    def _():
        ext[tokens : tokens + rim, :] = jnp.zeros((rim, width), F32)

    def conv_tile(index, carry):
        there = tile(index, 128)
        chunk = 64
        for start in range(0, tokens, chunk):
            value = jnp.zeros((chunk, 128), F32)
            for lag in range(lag_count):
                value = value + taps_ref[lag : lag + 1, there] * ext[start + lag : start + lag + chunk, there]
            gconv_ref[start : start + chunk, there] = value.astype(BF)
        return carry

    lax.fori_loop(0, width // 128, conv_tile, 0)

    @pl.when(group > 0)
    def _():
        halo().wait_send()

    for copy in outgoing:
        copy.wait_send()


def on_device(
    moe_in, cotangent, routes, route_weight, w_gate, w_up, w_down,
    conv_pre, norm_mean, norm_rstd, ln_gain, ln_shift, taps, w_proj,
):
    groups, lanes = (lax.axis_size("sp"), lax.axis_size("tp"))
    chips = lanes // 2
    across = 1 << (groups.bit_length() // 2 - 1)
    depth = groups // across
    group = lax.axis_index("sp")
    tokens, width = moe_in.shape
    channels = width * lanes
    hidden_units = w_gate.shape[1]
    cap = (5 * tokens // (2 * groups) + 15) // 16 * 16
    slots = groups * cap
    half_rows = slots // 2
    proj_rows = w_proj.shape[0]
    share = channels // groups
    piece_width = max(share, 128)
    rim = (taps.shape[0] - 1 + 7) // 8 * 8
    named = (routes ^ group).astype(F32)
    cols = jnp.concatenate([norm_mean[:, None], norm_rstd[:, None], named], axis=1)
    lines = jnp.concatenate([named.T, route_weight.T], axis=0)
    dma = pltpu.SemaphoreType.DMA
    vmem = pltpu.VMEM
    others = max(1, chips - 1)
    inside = pl.BlockSpec(memory_space=pltpu.VMEM)
    outside = pl.BlockSpec(memory_space=pl.ANY)
    return pl.pallas_call(
        functools.partial(layer_kernel, groups, lanes, across),
        out_shape=(
            jax.ShapeDtypeStruct(w_up.shape, BF),
            jax.ShapeDtypeStruct(w_down.shape, BF),
            jax.ShapeDtypeStruct((tokens, width), BF),
            jax.ShapeDtypeStruct((proj_rows, width), F32),
            jax.ShapeDtypeStruct((tokens, width), BF),
        ),
        in_specs=[inside] * 8 + [outside] * 4,
        out_specs=(inside,) * 5,
        scratch_shapes=[
            vmem((hidden_units, channels), BF), vmem((hidden_units, channels), BF), vmem((hidden_units, channels), BF),
            vmem((2, slots, width), BF), vmem((2, slots, channels), BF),
            vmem((hidden_units, half_rows), F32), vmem((hidden_units, half_rows), F32), vmem((hidden_units, half_rows), F32),
            vmem((hidden_units, slots), BF), vmem((hidden_units, slots), BF), vmem((hidden_units, slots), BF),
            vmem((slots, channels), BF), vmem((chips, slots, width), BF),
            vmem((others, slots, width), BF), vmem((others, slots, width), BF),
            vmem((slots, width), BF), vmem((slots, width), BF), vmem((tokens, slots), BF),
            vmem((groups, proj_rows + tokens, width), BF), vmem((tokens, channels), BF),
            vmem((groups, tokens, piece_width), BF),
            vmem((tokens, width), F32), vmem((tokens, width), F32),
            vmem((16, tokens), F32), vmem((lanes, 16, tokens), F32), vmem((tokens + rim, width), F32),
            dma((4,)), dma((groups,)), dma((groups,)),
            dma((groups, chips)), dma((groups, chips)), dma((groups, chips)), dma((groups, chips)),
            dma((2, chips)), dma((2, chips)), dma((groups, chips)), dma((groups, chips)),
            dma((groups,)), dma((groups,)),
            dma((2, 2, depth)), dma((2, 2, depth)), dma((2, 2 * depth, across)), dma((2, 2 * depth, across)),
            dma((chips,)), dma((chips,)), dma((chips,)), dma((chips,)),
            dma((groups,)), dma((groups,)), dma((lanes,)), dma((lanes,)), dma, dma,
        ],
        compiler_params=pltpu.CompilerParams(
            collective_id=1, has_side_effects=True, vmem_limit_bytes=60 * 1024 * 1024
        ),
    )(
        moe_in, cotangent, cols, lines, conv_pre, ln_gain[None, :], ln_shift[None, :], taps,
        w_gate, w_up, w_down, w_proj,
    )


def solution(mesh):
    placed = (
        P("sp", "tp"), P("sp", "tp"), P("sp", None), P("sp", None),
        P("sp", "tp", None), P("sp", "tp", None), P("sp", "tp", None),
        P("sp", "tp"), P("sp"), P("sp"), P("tp"), P("tp"), P(None, "tp"), P("sp", "tp"),
    )
    return jax.shard_map(
        on_device,
        mesh=mesh,
        in_specs=placed,
        out_specs=(
            P("sp", "tp", None), P("sp", "tp", None), P("sp", "tp"), P("sp", "tp"), P("sp", "tp"),
        ),
        check_vma=False,
    )
```

profile of v0, /device:TPU:0, one launch (start us, length us, event | category | flops | bytes accessed | tf_op | source)
XLA Modules:
  0.0 126.7 jit_solution(9531721045612245136)
XLA Ops:
  0.6 0.7 fusion
  1.3 0.7 xor_convert_fusion
  2.0 0.7 pad_maximum_fusion
  2.7 1.3 %pad_maximum_fusion.1.lines_ref = f32[4,192]{1,0:T(4,128)} fusion(f32[2,192]{1,0:T(2,128)} %bitcast.9, f32[2,192]{1,0:T(2,128)S(1)} %fusion), kind=kLoop, calls=%fused_computation.1 | loop fusion | flops 768 | bytes 6144 | tf_op jit(solution)/shard_map/concatenate | solution.py:541
  4.0 0.8 copy.19.cols_ref
  4.8 113.4 %shard_map.173 = (bf16[1,896,2048]{2,1,0:T(8,128)(2,1)}, bf16[1,896,2048]{2,1,0:T(8,128)(2,1)}, bf16[192,512]{1,0:T(8,128)(2,1)}, f32[256,512]{1,0:T(8,128)}, bf16[192,512]{1,0:T(8,128)(2,1)}) custom-call(bf16[192,512]{1,0:T(8,128)(2,1)} %moe_ref.1, bf16[192,512]{1,0:T(8,128)(2,1)} %cot_ref.1, f32[192,4]{1,0:T(8,128)} %copy.19.cols_ref, ...), custom_call_target="tpu_custom_call" | custom-call | tf_op jit(solution)/shard_map/pallas_call | solution.py:547
  118.2 0.0 copy-start
  118.2 4.5 %copy.25 = bf16[1,896,2048]{2,1,0:T(8,128)(2,1)} copy(bf16[1,896,2048]{2,1,0:T(8,128)(2,1)} %get-tuple-element.10) | data formatting | bytes 7340032
  122.7 0.0 copy-done
  122.7 0.0 copy-start.3
  122.7 0.0 copy-start.1
  122.7 0.0 copy-start.2
  122.7 1.8 %copy.26 = bf16[1,896,2048]{2,1,0:T(8,128)(2,1)} copy(bf16[1,896,2048]{2,1,0:T(8,128)(2,1)S(1)} %copy-done) | data formatting | bytes 7340032
  124.6 0.0 copy-done.3
  124.6 0.7 copy.27
  125.3 0.0 copy-done.1
  125.3 0.8 copy.28
  126.0 0.0 copy-done.2
  126.1 0.7 copy.29
Async XLA Ops:
  118.2 4.5 %copy-start = (bf16[1,896,2048]{2,1,0:T(8,128)(2,1)S(1)}, bf16[1,896,2048]{2,1,0:T(8,128)(2,1)}, u32[]{:S(2)}) copy-start(bf16[1,896,2048]{2,1,0:T(8,128)(2,1)} %get-tuple-element.11) | copy-start | bytes 11010052
  122.7 1.9 %copy-start.3 = (bf16[192,512]{1,0:T(8,128)(2,1)S(1)}, bf16[192,512]{1,0:T(8,128)(2,1)}, u32[]{:S(2)}) copy-start(bf16[192,512]{1,0:T(8,128)(2,1)} %get-tuple-element.12) | copy-start | bytes 589828
  122.7 2.5 %copy-start.1 = (f32[256,512]{1,0:T(8,128)S(1)}, f32[256,512]{1,0:T(8,128)}, u32[]{:S(2)}) copy-start(f32[256,512]{1,0:T(8,128)} %get-tuple-element.13) | copy-start | bytes 1572868
  122.7 3.3 %copy-start.2 = (bf16[192,512]{1,0:T(8,128)(2,1)S(1)}, bf16[192,512]{1,0:T(8,128)(2,1)}, u32[]{:S(2)}) copy-start(bf16[192,512]{1,0:T(8,128)(2,1)} %get-tuple-element.14) | copy-start | bytes 589828
where the time goes:
time: 127 us
  Pallas kernels  113 us (89%)
  local copies, waits for them, and re-layouts  9.29 us (7%)
  other arithmetic  3.36 us (3%)
    pallas_call x1, Pallas kernels, on_device(): pl.pallas_call(functools.partial(layer_kernel, groups, lanes, across), ou...  113 us
    unnamed x13, local copies, waits for them, and re-layouts  8.52 us

commit v1 on v0

--- a/solution.py
+++ b/solution.py
@@ -39,14 +39,14 @@
 
 def layer_kernel(
     groups, lanes, across,
-    moe_ref, cot_ref, cols_ref, lines_ref, conv_ref, gain_ref, shift_ref, taps_ref,
+    moe_ref, cot_ref, route_ref, weight_ref, mean_ref, rstd_ref, conv_ref, gain_ref, shift_ref, taps_ref,
     gate_hbm, up_hbm, down_hbm, proj_hbm,
     gup_ref, gdown_ref, gstream_ref, gproj_ref, gconv_ref,
     gate_w, up_w, down_w, send, rows, work_a, work_b, work_c, hid, upg, gtg,
     part, half, summed, arrived, total, returned, chosen_back, gathered, mix, pieces,
-    normed_s, slope_s, stat_out, stat_in, ext,
+    lines_s, normed_s, slope_s, stat_out, stat_in, ext,
     load_sem, dsp_s, dsp_r, dy_s, dy_r, dc_s, dc_r, sw_s, sw_r, cy_s, cy_r, csp_s, csp_r,
-    az_s, az_r, ax_s, ax_r, ty_s, ty_r, tc_s, tc_r, p_s, p_r, st_s, st_r, halo_s, halo_r,
+    az_s, az_r, ax_s, ax_r, ty_s, ty_r, tc_s, tc_r, p_s, p_r, py_s, py_r, pc_s, pc_r, st_s, st_r, halo_s, halo_r,
 ):
     group, lane = (lax.axis_index("sp"), lax.axis_index("tp"))
     chips = lanes // 2
@@ -58,9 +58,7 @@
     hidden_units = gate_w.shape[0]
     slots = groups * (rows.shape[1] // groups)
     cap = slots // groups
-    halves = 2
-    per_half = groups // halves
-    half_rows = slots // halves
+    chunks = ((0, 3 * groups // 4), (3 * groups // 4, groups))
     proj_rows = proj_hbm.shape[0]
     lag_count = taps_ref.shape[0]
     partner = (group, flipped(lane, 1))
@@ -87,26 +85,39 @@
     for copy in loads:
         copy.start()
 
-    named_line = (lines_ref[0:1, :], lines_ref[1:2, :])
-    weight_line = (lines_ref[2:3, :], lines_ref[3:4, :])
-    named_col = (cols_ref[:, 2:3], cols_ref[:, 3:4])
+    lines_s[...] = jnp.zeros(lines_s.shape, F32)
+    lines_s[0:2, 0:tokens] = (route_ref[...] ^ group).astype(F32)
+    lines_s[2:3, 0:tokens] = mean_ref[...]
+    lines_s[3:4, 0:tokens] = rstd_ref[...]
+    named_line = (lines_s[0:1, 0:tokens], lines_s[1:2, 0:tokens])
+    weight_line = (weight_ref[0:1, :], weight_ref[1:2, :])
+    columns = lines_s[...].T
+    named_col = (columns[0:tokens, 0:1], columns[0:tokens, 1:2])
+    mean_col, rstd_col = (columns[0:tokens, 2:3], columns[0:tokens, 3:4])
     down_iota = lax.broadcasted_iota(jnp.int32, (tokens, tokens), 0)
     over_iota = lax.broadcasted_iota(jnp.int32, (tokens, tokens), 1)
-    place = lax.broadcasted_iota(jnp.int32, (slots, tokens), 0).astype(F32)
-    matches, slot_weight = ([], 0.0)
+    targets = []
     for choice in range(2):
         same = jnp.where(named_col[0] == named_line[choice], 1.0, 0.0) + jnp.where(
             named_col[1] == named_line[choice], 1.0, 0.0
         )
         rank = jnp.sum(jnp.where(down_iota < over_iota, same, 0.0), axis=0, keepdims=True)
-        match = place == named_line[choice] * float(cap) + rank
-        matches.append(match)
-        slot_weight = slot_weight + jnp.sum(
-            jnp.where(match, weight_line[choice], 0.0), axis=1, keepdims=True
+        targets.append(named_line[choice] * float(cap) + rank)
+
+    def fill(low, high):
+        here = slice(low * cap, high * cap)
+        count = (high - low) * cap
+        place = lax.broadcasted_iota(jnp.int32, (count, tokens), 0).astype(F32) + float(low * cap)
+        first, second = (place == targets[0], place == targets[1])
+        slot_weight = jnp.sum(
+            jnp.where(first, weight_line[0], 0.0) + jnp.where(second, weight_line[1], 0.0),
+            axis=1, keepdims=True,
         )
-    chosen = jnp.where(matches[0] | matches[1], 1.0, 0.0).astype(BF)
-    send[0] = nn(chosen, moe_ref[...]).astype(BF)
-    send[1] = (slot_weight * nn(chosen, cot_ref[...])).astype(BF)
+        chosen = jnp.where(first | second, 1.0, 0.0).astype(BF)
+        send[0, here, :] = nn(chosen, moe_ref[...]).astype(BF)
+        send[1, here, :] = (slot_weight * nn(chosen, cot_ref[...])).astype(BF)
+
+    fill(0, groups // 2)
     rows[0, 0:cap, mine] = send[0, 0:cap, :]
     rows[1, 0:cap, mine] = send[1, 0:cap, :]
 
@@ -142,12 +153,18 @@
                 at_slot(step, peer), at_slot(step, peer), dc_s.at[step, turn], dc_r.at[step, turn], partner
             ))
 
-    forward(0)
-    for step in range(1, groups):
+    def dispatch(step):
         dispatched[step] = go(remote(
             send.at[:, pl.ds(step * cap, cap)], at_slot(step, lane),
             dsp_s.at[step], dsp_r.at[step], (flipped(group, step), lane),
         ))
+
+    forward(0)
+    for step in range(1, groups // 2):
+        dispatch(step)
+    fill(groups // 2, groups)
+    for step in range(groups // 2, groups):
+        dispatch(step)
 
     bounds = ((0, proj_rows), (proj_rows, tokens))
 
@@ -183,11 +200,13 @@
             ))
         return copies
 
-    def gather_own(kind):
+    def gather_along(kind):
         for way in range(2):
             @pl.when(along_valid(way, 0))
             def _():
                 along(kind, way, 0).start()
+
+    def gather_sideways(kind):
         for copy in sideways(kind, 0, level):
             copy.start()
 
@@ -222,12 +241,14 @@
                         copy.wait()
 
     loads[0].wait()
-    gather_own(0)
-
-    normed = (conv_ref[...].astype(F32) - cols_ref[:, 0:1]) * cols_ref[:, 1:2]
+    gather_along(0)
+    gather_sideways(0)
+
+    normed = (conv_ref[...].astype(F32) - mean_col) * rstd_col
     pre_act = normed * gain_ref[...] + shift_ref[...]
     act_sigmoid = jax.nn.sigmoid(pre_act)
     gathered[group, proj_rows : proj_rows + tokens, :] = (pre_act * act_sigmoid).astype(BF)
+    gather_sideways(1)
     normed_s[...] = normed
     slope_s[...] = act_sigmoid * (1.0 + pre_act * (1.0 - act_sigmoid)) * gain_ref[...]
     back_place = lax.broadcasted_iota(jnp.int32, (tokens, slots), 1).astype(F32)
@@ -241,16 +262,19 @@
         back = match if back is None else back | match
     chosen_back[...] = jnp.where(back, 1.0, 0.0).astype(BF)
 
-    def of_half(part_index):
-        return slice(part_index * half_rows, (part_index + 1) * half_rows)
+    def of_chunk(part_index):
+        return slice(chunks[part_index][0] * cap, chunks[part_index][1] * cap)
 
     def activate(part_index):
-        here = of_half(part_index)
+        here = of_chunk(part_index)
         step_rows = 64
+        count = here.stop - here.start
 
         def body(index, carry):
             there = tile(index, step_rows)
-            gate_pre, up_pre, hidden_grad = (work_a[there, :], work_b[there, :], work_c[there, :])
+            gate_pre, up_pre, hidden_grad = (
+                work_a[there, 0:count], work_b[there, 0:count], work_c[there, 0:count]
+            )
             gate_sigmoid = jax.nn.sigmoid(gate_pre)
             gate_active = gate_pre * gate_sigmoid
             hid[there, here] = (gate_active * up_pre).astype(BF)
@@ -263,7 +287,7 @@
         lax.fori_loop(0, hidden_units // step_rows, body, 0)
 
     def partial_columns(part_index, lane_index):
-        here = of_half(part_index)
+        here = of_chunk(part_index)
         there = tile(lane_index, width)
         value = tn(gtg[:, here], gate_w[:, there]) + tn(upg[:, here], up_w[:, there])
         part[here, there] = value.astype(BF)
@@ -272,7 +296,7 @@
 
     def swap(part_index, turn):
         away = flipped(lane, 2 * turn + 1)
-        here = pl.ds(part_index * half_rows, half_rows)
+        here = pl.ds(chunks[part_index][0] * cap, (chunks[part_index][1] - chunks[part_index][0]) * cap)
         swaps[part_index, turn] = go(remote(
             part.at[here, tile(away, width)], half.at[turn, here],
             sw_s.at[part_index, turn], sw_r.at[part_index, turn], partner,
@@ -288,7 +312,7 @@
         for turn in range(1, chips):
             away = flipped(lane, 2 * turn)
             swaps[part_index, turn].wait_recv()
-            for step in range(part_index * per_half, (part_index + 1) * per_half):
+            for step in range(*chunks[part_index]):
                 here = slice(step * cap, (step + 1) * cap)
                 summed[turn - 1, here, :] = (
                     part[here, tile(away, width)].astype(F32) + half[turn, here, :].astype(F32)
@@ -300,7 +324,7 @@
 
     def send_home(part_index):
         swaps[part_index, 0].wait_recv()
-        for step in range(part_index * per_half, (part_index + 1) * per_half):
+        for step in range(*chunks[part_index]):
             here = slice(step * cap, (step + 1) * cap)
             value = part[here, mine].astype(F32) + half[0, here, :].astype(F32)
             for turn in range(1, chips):
@@ -315,58 +339,59 @@
             else:
                 returned[here, :] = value.astype(BF)
 
-    for step in range(1, per_half):
+    def first_matmuls(part_index, between):
+        here = of_chunk(part_index)
+        count = here.stop - here.start
+        for work, weight, source in ((work_a, gate_w, 0), (work_b, up_w, 0), (work_c, down_w, 1)):
+            work[:, 0:count] = nt(weight[...], rows[source, here, :])
+            between.pop(0)()
+
+    def advance(low, high):
+        for step in range(low, high):
+            dispatched[step].wait_recv()
+            forward(step)
+            relay(step - 1)
+
+    edge = chunks[0][1]
+    advance(1, edge)
+    middle = (edge + groups) // 2
+    for step in range(edge, middle):
         dispatched[step].wait_recv()
         forward(step)
-        relay(step - 1)
-    far = list(range(per_half, groups))
-    quarter = max(1, len(far) // 4)
-    for step in far[:quarter]:
-        dispatched[step].wait_recv()
-        forward(step)
-    relay(per_half - 1)
-    for step in range(per_half):
+    relay(edge - 1)
+    for step in range(edge):
         for turn in range(chips):
             shared[step, turn].wait_recv()
-    near = of_half(0)
     for copy in loads[1:]:
         copy.wait()
-    work_a[...] = nt(gate_w[...], rows[0, near, :])
-    for step in far[quarter : 2 * quarter]:
-        dispatched[step].wait_recv()
-        forward(step)
-    work_b[...] = nt(up_w[...], rows[0, near, :])
-    work_c[...] = nt(down_w[...], rows[1, near, :])
-    for step in far[2 * quarter : 3 * quarter]:
-        dispatched[step].wait_recv()
-        forward(step)
+
+    def last_forward():
+        for step in range(middle, groups):
+            dispatched[step].wait_recv()
+            forward(step)
+
+    def nothing():
+        return None
+
+    first_matmuls(0, [last_forward, nothing, nothing])
     activate(0)
-    for step in far[:quarter]:
+    for step in range(edge, groups):
         relay(step)
     partials(0)
-    for step in far[3 * quarter :]:
-        dispatched[step].wait_recv()
-        forward(step)
-    for step in far[quarter:]:
-        relay(step)
+    gather_hop(0, 0)
     chip_sums(0)
-
-    for step in far:
+    for step in range(edge, groups):
         for turn in range(chips):
             shared[step, turn].wait_recv()
-    beyond = of_half(1)
-    work_a[...] = nt(gate_w[...], rows[0, beyond, :])
-    gather_hop(0, 0)
-    work_b[...] = nt(up_w[...], rows[0, beyond, :])
-    work_c[...] = nt(down_w[...], rows[1, beyond, :])
+    first_matmuls(1, [nothing, lambda: send_home(0), nothing])
     activate(1)
-    send_home(0)
     partials(1)
+    gather_hop(0, 1)
     chip_sums(1)
-    for hop in range(1, depth - 1):
+    for hop in range(2, depth - 1):
         gather_hop(0, hop)
     send_home(1)
-    gather_own(1)
+    gather_along(1)
 
     span = min(channels, 512)
 
@@ -381,7 +406,6 @@
         return carry
 
     lax.fori_loop(0, channels // span, down_tile, 0)
-    gather_hop(1, 0)
     lax.fori_loop(0, channels // span, up_tile, 0)
 
     for step in range(1, groups):
@@ -402,27 +426,41 @@
         tp_shared[turn] = go(remote(
             mix.at[:, theirs], mix.at[:, theirs], tc_s.at[turn], tc_r.at[turn], partner
         ))
-    gather_rest(0)
     for turn in range(chips):
         tp_shared[turn].wait_recv()
-    for hop in range(1, depth - 1):
-        gather_hop(1, hop)
 
     share = channels // groups
-    piece_width = pieces.shape[2]
+    piece_width = pieces.shape[3]
+    quarter = tokens // 4
+    place_of_four = lax.rem(lane, 4)
 
     def piece_of(owner):
         if share == piece_width:
             return tile(owner, share)
         return tile(lax.div(owner * share, piece_width), piece_width)
 
-    travelling = {}
+    travelling, piece_across, piece_shared = ({}, {}, {})
     for step in range(1, groups):
         owner = flipped(group, step)
         travelling[step] = go(remote(
-            mix.at[:, piece_of(owner)], pieces.at[step], p_s.at[step], p_r.at[step], (owner, lane)
+            mix.at[tile(place_of_four, quarter), piece_of(owner)], pieces.at[step, place_of_four],
+            p_s.at[step], p_r.at[step], (owner, lane),
         ))
 
+    def piece_forward(step):
+        travelling[step].wait_recv()
+        here = pieces.at[step, place_of_four]
+        piece_across[step] = go(remote(
+            here, here, py_s.at[step], py_r.at[step], (group, flipped(lane, 2))
+        ))
+        piece_shared[step, 0] = go(remote(here, here, pc_s.at[step, 0], pc_r.at[step, 0], partner))
+
+    def piece_relay(step):
+        piece_across[step].wait_recv()
+        here = pieces.at[step, flipped(place_of_four, 2)]
+        piece_shared[step, 1] = go(remote(here, here, pc_s.at[step, 1], pc_r.at[step, 1], partner))
+
+    gather_rest(0)
     whole_proj = gathered[:, 0:proj_rows, :].reshape(groups * proj_rows, width)
     normed_grad = nn(mix[...], whole_proj) * slope_s[...]
     weighted = normed_grad * normed_s[...]
@@ -441,6 +479,9 @@
         stats.append(go(remote(
             stat_out, stat_in.at[step], st_s.at[step], st_r.at[step], (group, flipped(lane, step))
         )))
+    for step in range(1, groups // 2):
+        piece_forward(step)
+    gather_hop(1, 0)
     all_stat = own_stat
     for step in range(1, lanes):
         stats[step - 1].wait_recv()
@@ -455,9 +496,7 @@
         chooser = jnp.where(pick == number, 1.0, 0.0).astype(BF)
         return tn(high, chooser) + tn(middle, chooser) + tn(low, chooser)
 
-    ext[0:tokens, :] = cols_ref[:, 1:2] * (
-        normed_grad - spread_line(0) - normed_s[...] * spread_line(1)
-    )
+    first_line, second_line = (spread_line(0), spread_line(1))
     rim = ext.shape[0] - tokens
 
     def halo():
@@ -465,9 +504,44 @@
             ext.at[pl.ds(0, rim)], ext.at[pl.ds(tokens, rim)], halo_s, halo_r, (group - 1, lane)
         )
 
+    def conv_gradient(here):
+        ext[here, :] = rstd_col[here] * (
+            normed_grad[here] - first_line[here] - normed_s[here, :] * second_line[here]
+        )
+
+    conv_gradient(slice(0, rim))
+
     @pl.when(group > 0)
     def _():
         halo().start()
+
+    conv_gradient(slice(rim, tokens))
+    for step in range(groups // 2, groups):
+        piece_forward(step)
+    for hop in range(1, depth - 1):
+        gather_hop(1, hop)
+    for step in range(1, groups):
+        piece_relay(step)
+
+    @pl.when(group < groups - 1)
+    def _():
+        halo().wait_recv()
+
+    @pl.when(group == groups - 1)
+    def _():
+        ext[tokens : tokens + rim, :] = jnp.zeros((rim, width), F32)
+
+    def conv_tile(index, carry):
+        there = tile(index, 128)
+        chunk = 64
+        for start in range(0, tokens, chunk):
+            value = jnp.zeros((chunk, 128), F32)
+            for lag in range(lag_count):
+                value = value + taps_ref[lag : lag + 1, there] * ext[start + lag : start + lag + chunk, there]
+            gconv_ref[start : start + chunk, there] = value.astype(BF)
+        return carry
+
+    lax.fori_loop(0, width // 128, conv_tile, 0)
 
     def piece_value(value):
         if share == piece_width:
@@ -479,35 +553,14 @@
             result = jnp.where(which == index, value[:, index * share : (index + 1) * share], result)
         return result
 
-    for hop in range(depth - 1, depth - 1):
-        gather_hop(1, hop)
     gather_rest(1)
     gproj = tn(piece_value(mix[:, piece_of(group)]), gathered[group, proj_rows : proj_rows + tokens, :])
     for step in range(1, groups):
-        travelling[step].wait_recv()
+        for turn in range(2):
+            piece_shared[step, turn].wait_recv()
         owner = flipped(group, step)
-        gproj = gproj + tn(piece_value(pieces[step]), gathered[owner, proj_rows : proj_rows + tokens, :])
+        gproj = gproj + tn(piece_value(pieces[step].reshape(tokens, piece_width)), gathered[owner, proj_rows : proj_rows + tokens, :])
     gproj_ref[...] = gproj
-
-    @pl.when(group < groups - 1)
-    def _():
-        halo().wait_recv()
-
-    @pl.when(group == groups - 1)
-    def _():
-        ext[tokens : tokens + rim, :] = jnp.zeros((rim, width), F32)
-
-    def conv_tile(index, carry):
-        there = tile(index, 128)
-        chunk = 64
-        for start in range(0, tokens, chunk):
-            value = jnp.zeros((chunk, 128), F32)
-            for lag in range(lag_count):
-                value = value + taps_ref[lag : lag + 1, there] * ext[start + lag : start + lag + chunk, there]
-            gconv_ref[start : start + chunk, there] = value.astype(BF)
-        return carry
-
-    lax.fori_loop(0, width // 128, conv_tile, 0)
 
     @pl.when(group > 0)
     def _():
@@ -525,20 +578,17 @@
     chips = lanes // 2
     across = 1 << (groups.bit_length() // 2 - 1)
     depth = groups // across
-    group = lax.axis_index("sp")
     tokens, width = moe_in.shape
     channels = width * lanes
     hidden_units = w_gate.shape[1]
     cap = (5 * tokens // (2 * groups) + 15) // 16 * 16
     slots = groups * cap
-    half_rows = slots // 2
+    chunk_rows = 3 * groups // 4 * cap
     proj_rows = w_proj.shape[0]
     share = channels // groups
     piece_width = max(share, 128)
     rim = (taps.shape[0] - 1 + 7) // 8 * 8
-    named = (routes ^ group).astype(F32)
-    cols = jnp.concatenate([norm_mean[:, None], norm_rstd[:, None], named], axis=1)
-    lines = jnp.concatenate([named.T, route_weight.T], axis=0)
+    vmem_limit = 48 * 1024 * 1024
     dma = pltpu.SemaphoreType.DMA
     vmem = pltpu.VMEM
     others = max(1, chips - 1)
@@ -547,25 +597,25 @@
     return pl.pallas_call(
         functools.partial(layer_kernel, groups, lanes, across),
         out_shape=(
-            jax.ShapeDtypeStruct(w_up.shape, BF),
-            jax.ShapeDtypeStruct(w_down.shape, BF),
-            jax.ShapeDtypeStruct((tokens, width), BF),
-            jax.ShapeDtypeStruct((proj_rows, width), F32),
-            jax.ShapeDtypeStruct((tokens, width), BF),
+            vmem(w_up.shape, BF),
+            vmem(w_down.shape, BF),
+            vmem((tokens, width), BF),
+            vmem((proj_rows, width), F32),
+            vmem((tokens, width), BF),
         ),
-        in_specs=[inside] * 8 + [outside] * 4,
+        in_specs=[inside] * 10 + [outside] * 4,
         out_specs=(inside,) * 5,
         scratch_shapes=[
             vmem((hidden_units, channels), BF), vmem((hidden_units, channels), BF), vmem((hidden_units, channels), BF),
             vmem((2, slots, width), BF), vmem((2, slots, channels), BF),
-            vmem((hidden_units, half_rows), F32), vmem((hidden_units, half_rows), F32), vmem((hidden_units, half_rows), F32),
+            vmem((hidden_units, chunk_rows), F32), vmem((hidden_units, chunk_rows), F32), vmem((hidden_units, chunk_rows), F32),
             vmem((hidden_units, slots), BF), vmem((hidden_units, slots), BF), vmem((hidden_units, slots), BF),
             vmem((slots, channels), BF), vmem((chips, slots, width), BF),
             vmem((others, slots, width), BF), vmem((others, slots, width), BF),
             vmem((slots, width), BF), vmem((slots, width), BF), vmem((tokens, slots), BF),
             vmem((groups, proj_rows + tokens, width), BF), vmem((tokens, channels), BF),
-            vmem((groups, tokens, piece_width), BF),
-            vmem((tokens, width), F32), vmem((tokens, width), F32),
+            vmem((groups, 4, tokens // 4, piece_width), BF),
+            vmem((128, (tokens + 127) // 128 * 128), F32), vmem((tokens, width), F32), vmem((tokens, width), F32),
             vmem((16, tokens), F32), vmem((lanes, 16, tokens), F32), vmem((tokens + rim, width), F32),
             dma((4,)), dma((groups,)), dma((groups,)),
             dma((groups, chips)), dma((groups, chips)), dma((groups, chips)), dma((groups, chips)),
@@ -573,13 +623,14 @@
             dma((groups,)), dma((groups,)),
             dma((2, 2, depth)), dma((2, 2, depth)), dma((2, 2 * depth, across)), dma((2, 2 * depth, across)),
             dma((chips,)), dma((chips,)), dma((chips,)), dma((chips,)),
-            dma((groups,)), dma((groups,)), dma((lanes,)), dma((lanes,)), dma, dma,
+            dma((groups,)), dma((groups,)), dma((groups,)), dma((groups,)), dma((groups, 2)), dma((groups, 2)),
+            dma((lanes,)), dma((lanes,)), dma, dma,
         ],
         compiler_params=pltpu.CompilerParams(
-            collective_id=1, has_side_effects=True, vmem_limit_bytes=60 * 1024 * 1024
+            collective_id=1, has_side_effects=True, vmem_limit_bytes=vmem_limit
         ),
     )(
-        moe_in, cotangent, cols, lines, conv_pre, ln_gain[None, :], ln_shift[None, :], taps,
+        moe_in, cotangent, routes.T, route_weight.T, norm_mean[None, :], norm_rstd[None, :], conv_pre, ln_gain[None, :], ln_shift[None, :], taps,
         w_gate, w_up, w_down, w_proj,
     )
 

time: 127 us -> 110 us (0.87)
  Pallas kernels: 113 us -> 103 us
  local copies, waits for them, and re-layouts: 9.29 us -> 5.82 us
  other arithmetic: 3.36 us -> 0 us
    pallas_call x1, Pallas kernels: 113 us -> 103 us  [on_device(): pl.pallas_call(functools.partial(layer_kernel, groups, lanes, across), ou...]
    unnamed x13 -> x5, local copies, waits for them, and re-layouts: 8.52 us -> 5.82 us
    concatenate x2 -> x0, other arithmetic: 1.99 us -> none  [the longest x1 1.28 us: on_device(): lines = jnp.concatenate([named.T, route_weight.T], axis=0)]
where the time goes in v1:
time: 110 us
  Pallas kernels  103 us (94%)
  local copies, waits for them, and re-layouts  5.82 us (5%)
    pallas_call x1, Pallas kernels, on_device(): pl.pallas_call(functools.partial(layer_kernel, groups, lanes, across), ou...  103 us
    unnamed x5, local copies, waits for them, and re-layouts  5.82 us

profile of v1, /device:TPU:0, one launch (start us, length us, event | category | flops | bytes accessed | tf_op | source)
XLA Modules:
  0.0 109.7 jit_solution(9446353448442716981)
XLA Ops:
  0.6 103.2 %shard_map.173 = (bf16[1,896,2048]{2,1,0:T(8,128)(2,1)S(1)}, bf16[1,896,2048]{2,1,0:T(8,128)(2,1)S(1)}, bf16[192,512]{1,0:T(8,128)(2,1)S(1)}, f32[256,512]{1,0:T(8,128)S(1)}, bf16[192,512]{1,0:T(8,128)(2,1)S(1)}) custom-call(bf16[192,512]{1,0:T(8,128)(2,1)} %moe_ref.1, bf16[192,512]{1,0:T(8,128)(2,1)} %cot_ref.1, s32[2,192]{1,0:T(2,128)} %bitcast.6, ...), custom_call_target="tpu_custom_call" | custom-call | tf_op jit(solution)/shard_map/pallas_call | solution.py:597
  103.8 1.8 %copy.24 = bf16[1,896,2048]{2,1,0:T(8,128)(2,1)} copy(bf16[1,896,2048]{2,1,0:T(8,128)(2,1)S(1)} %get-tuple-element.5) | data formatting | bytes 7340032
  105.7 0.7 copy.26
  106.3 0.7 copy.28
  107.0 0.8 copy.27
  107.8 1.8 %copy.25 = bf16[1,896,2048]{2,1,0:T(8,128)(2,1)} copy(bf16[1,896,2048]{2,1,0:T(8,128)(2,1)S(1)} %get-tuple-element.6) | data formatting | bytes 7340032

commit v2 on v1

--- a/solution.py
+++ b/solution.py
@@ -58,7 +58,7 @@
     hidden_units = gate_w.shape[0]
     slots = groups * (rows.shape[1] // groups)
     cap = slots // groups
-    chunks = ((0, 3 * groups // 4), (3 * groups // 4, groups))
+    chunks = ((0, groups // 2), (groups // 2, 3 * groups // 4), (3 * groups // 4, groups))
     proj_rows = proj_hbm.shape[0]
     lag_count = taps_ref.shape[0]
     partner = (group, flipped(lane, 1))
@@ -138,7 +138,7 @@
     def forward(step):
         for turn in range(1, chips):
             crossed[step, turn] = go(remote(
-                at_slot(step, lane), at_slot(step, lane), dy_s.at[step, turn], dy_r.at[step, turn],
+                at_slot(step, lane), at_slot(step, lane), dy_s.at[step, turn - 1], dy_r.at[step, turn - 1],
                 (group, flipped(lane, 2 * turn)),
             ))
         shared[step, 0] = go(remote(
@@ -163,7 +163,7 @@
     for step in range(1, groups // 2):
         dispatch(step)
     fill(groups // 2, groups)
-    for step in range(groups // 2, groups):
+    for step in range(groups // 2, 3 * groups // 4):
         dispatch(step)
 
     bounds = ((0, proj_rows), (proj_rows, tokens))
@@ -195,14 +195,18 @@
         for turn in range(1, across):
             here = block(owner_level, column, kind)
             copies.append(remote(
-                here, here, ax_s.at[kind, event, turn], ax_r.at[kind, event, turn],
+                here, here, ax_s.at[kind, event, turn - 1], ax_r.at[kind, event, turn - 1],
                 (level * across + flipped(column, turn), lane),
             ))
         return copies
 
-    def gather_along(kind):
+    def over_middle(way, source_level, wanted):
+        edge_level = depth // 2 - 1 + way
+        return (source_level == edge_level) if wanted else (source_level != edge_level)
+
+    def gather_along(kind, middle):
         for way in range(2):
-            @pl.when(along_valid(way, 0))
+            @pl.when(along_valid(way, 0) & over_middle(way, level, middle))
             def _():
                 along(kind, way, 0).start()
 
@@ -210,11 +214,14 @@
         for copy in sideways(kind, 0, level):
             copy.start()
 
-    def gather_hop(kind, hop):
+    def gather_hop(kind, hop, middle=None):
         for way in range(2):
             sign = 1 - 2 * way
-
-            @pl.when(arrives_valid(way, hop))
+            due = arrives_valid(way, hop)
+            if middle is not None:
+                due = due & over_middle(way, level - sign, middle)
+
+            @pl.when(due)
             def _():
                 along(kind, way, hop).wait_recv()
                 if hop + 1 < depth - 1:
@@ -240,15 +247,11 @@
                     for copy in sideways(kind, 1 + 2 * hop + way, level - sign * (hop + 1)):
                         copy.wait()
 
-    loads[0].wait()
-    gather_along(0)
-    gather_sideways(0)
 
     normed = (conv_ref[...].astype(F32) - mean_col) * rstd_col
     pre_act = normed * gain_ref[...] + shift_ref[...]
     act_sigmoid = jax.nn.sigmoid(pre_act)
     gathered[group, proj_rows : proj_rows + tokens, :] = (pre_act * act_sigmoid).astype(BF)
-    gather_sideways(1)
     normed_s[...] = normed
     slope_s[...] = act_sigmoid * (1.0 + pre_act * (1.0 - act_sigmoid)) * gain_ref[...]
     back_place = lax.broadcasted_iota(jnp.int32, (tokens, slots), 1).astype(F32)
@@ -302,11 +305,13 @@
             sw_s.at[part_index, turn], sw_r.at[part_index, turn], partner,
         ))
 
-    def partials(part_index):
+    def partials(part_index, between):
         for turn in [*range(1, chips), 0]:
             partial_columns(part_index, flipped(lane, 2 * turn + 1))
             swap(part_index, turn)
             partial_columns(part_index, flipped(lane, 2 * turn))
+            if turn == 1:
+                between()
 
     def chip_sums(part_index):
         for turn in range(1, chips):
@@ -319,7 +324,7 @@
                 ).astype(BF)
                 back_across[step, turn] = go(remote(
                     summed.at[turn - 1, pl.ds(step * cap, cap)], arrived.at[turn - 1, pl.ds(step * cap, cap)],
-                    cy_s.at[step, turn], cy_r.at[step, turn], (group, away),
+                    cy_s.at[step, turn - 1], cy_r.at[step, turn - 1], (group, away),
                 ))
 
     def send_home(part_index):
@@ -350,48 +355,71 @@
         for step in range(low, high):
             dispatched[step].wait_recv()
             forward(step)
+            if step % 2:
+                dispatch(3 * groups // 4 + step // 2)
             relay(step - 1)
 
-    edge = chunks[0][1]
-    advance(1, edge)
-    middle = (edge + groups) // 2
-    for step in range(edge, middle):
-        dispatched[step].wait_recv()
-        forward(step)
-    relay(edge - 1)
-    for step in range(edge):
-        for turn in range(chips):
-            shared[step, turn].wait_recv()
+    def pass_on(low, high):
+        for step in range(low, high):
+            dispatched[step].wait_recv()
+            forward(step)
+
+    def relays(low, high):
+        for step in range(low, high):
+            relay(step)
+
+    def complete(part_index):
+        for step in range(*chunks[part_index]):
+            for turn in range(chips):
+                shared[step, turn].wait_recv()
+
+    def nothing():
+        return None
+
+    first_edge, second_edge = (chunks[0][1], chunks[1][1])
+    first_half, second_half = ((first_edge + second_edge) // 2, (second_edge + groups) // 2)
+    advance(1, first_edge)
+    loads[0].wait()
+    for kind in range(2):
+        gather_along(kind, False)
+        gather_sideways(kind)
+    relays(first_edge - 1, first_edge)
+    complete(0)
+    pass_on(first_edge, first_half)
     for copy in loads[1:]:
         copy.wait()
-
-    def last_forward():
-        for step in range(middle, groups):
-            dispatched[step].wait_recv()
-            forward(step)
-
-    def nothing():
-        return None
-
-    first_matmuls(0, [last_forward, nothing, nothing])
+    gather_along(0, True)
+    first_matmuls(0, [lambda: pass_on(first_half, second_edge), nothing, lambda: pass_on(second_edge, second_half)])
     activate(0)
-    for step in range(edge, groups):
-        relay(step)
-    partials(0)
-    gather_hop(0, 0)
+    relays(first_edge, first_half)
+
+    def rest_of_dispatch():
+        pass_on(second_half, groups)
+        relays(first_half, second_edge)
+
+    partials(0, rest_of_dispatch)
+    relays(second_edge, second_half)
     chip_sums(0)
-    for step in range(edge, groups):
-        for turn in range(chips):
-            shared[step, turn].wait_recv()
-    first_matmuls(1, [nothing, lambda: send_home(0), nothing])
+    gather_hop(0, 0, False)
+    gather_along(1, True)
+    gather_hop(1, 0, False)
+    complete(1)
+    first_matmuls(1, [nothing, nothing, nothing])
+    relays(second_half, groups)
+    gather_hop(0, 0, True)
     activate(1)
-    partials(1)
+    partials(1, nothing)
+    chip_sums(1)
+    complete(2)
+    first_matmuls(2, [nothing, nothing, nothing])
     gather_hop(0, 1)
-    chip_sums(1)
-    for hop in range(2, depth - 1):
-        gather_hop(0, hop)
+    send_home(0)
+    activate(2)
     send_home(1)
-    gather_along(1)
+    gather_hop(1, 0, True)
+    partials(2, nothing)
+    chip_sums(2)
+    send_home(2)
 
     span = min(channels, 512)
 
@@ -407,6 +435,9 @@
 
     lax.fori_loop(0, channels // span, down_tile, 0)
     lax.fori_loop(0, channels // span, up_tile, 0)
+    for hop in range(2, depth - 1):
+        gather_hop(0, hop)
+    gather_hop(1, 1, True)
 
     for step in range(1, groups):
         homeward[step].wait_recv()
@@ -426,6 +457,7 @@
         tp_shared[turn] = go(remote(
             mix.at[:, theirs], mix.at[:, theirs], tc_s.at[turn], tc_r.at[turn], partner
         ))
+    gather_hop(1, 1, False)
     for turn in range(chips):
         tp_shared[turn].wait_recv()
 
@@ -479,9 +511,6 @@
         stats.append(go(remote(
             stat_out, stat_in.at[step], st_s.at[step], st_r.at[step], (group, flipped(lane, step))
         )))
-    for step in range(1, groups // 2):
-        piece_forward(step)
-    gather_hop(1, 0)
     all_stat = own_stat
     for step in range(1, lanes):
         stats[step - 1].wait_recv()
@@ -516,12 +545,10 @@
         halo().start()
 
     conv_gradient(slice(rim, tokens))
-    for step in range(groups // 2, groups):
-        piece_forward(step)
-    for hop in range(1, depth - 1):
+    for hop in range(2, depth - 1):
         gather_hop(1, hop)
     for step in range(1, groups):
-        piece_relay(step)
+        piece_forward(step)
 
     @pl.when(group < groups - 1)
     def _():
@@ -553,6 +580,8 @@
             result = jnp.where(which == index, value[:, index * share : (index + 1) * share], result)
         return result
 
+    for step in range(1, groups):
+        piece_relay(step)
     gather_rest(1)
     gproj = tn(piece_value(mix[:, piece_of(group)]), gathered[group, proj_rows : proj_rows + tokens, :])
     for step in range(1, groups):
@@ -583,7 +612,6 @@
     hidden_units = w_gate.shape[1]
     cap = (5 * tokens // (2 * groups) + 15) // 16 * 16
     slots = groups * cap
-    chunk_rows = 3 * groups // 4 * cap
     proj_rows = w_proj.shape[0]
     share = channels // groups
     piece_width = max(share, 128)
@@ -594,7 +622,7 @@
     others = max(1, chips - 1)
     inside = pl.BlockSpec(memory_space=pltpu.VMEM)
     outside = pl.BlockSpec(memory_space=pl.ANY)
-    return pl.pallas_call(
+    results = pl.pallas_call(
         functools.partial(layer_kernel, groups, lanes, across),
         out_shape=(
             vmem(w_up.shape, BF),
@@ -608,7 +636,7 @@
         scratch_shapes=[
             vmem((hidden_units, channels), BF), vmem((hidden_units, channels), BF), vmem((hidden_units, channels), BF),
             vmem((2, slots, width), BF), vmem((2, slots, channels), BF),
-            vmem((hidden_units, chunk_rows), F32), vmem((hidden_units, chunk_rows), F32), vmem((hidden_units, chunk_rows), F32),
+            vmem((hidden_units, slots // 2), F32), vmem((hidden_units, slots // 2), F32), vmem((hidden_units, slots // 2), F32),
             vmem((hidden_units, slots), BF), vmem((hidden_units, slots), BF), vmem((hidden_units, slots), BF),
             vmem((slots, channels), BF), vmem((chips, slots, width), BF),
             vmem((others, slots, width), BF), vmem((others, slots, width), BF),
@@ -618,10 +646,11 @@
             vmem((128, (tokens + 127) // 128 * 128), F32), vmem((tokens, width), F32), vmem((tokens, width), F32),
             vmem((16, tokens), F32), vmem((lanes, 16, tokens), F32), vmem((tokens + rim, width), F32),
             dma((4,)), dma((groups,)), dma((groups,)),
-            dma((groups, chips)), dma((groups, chips)), dma((groups, chips)), dma((groups, chips)),
-            dma((2, chips)), dma((2, chips)), dma((groups, chips)), dma((groups, chips)),
+            dma((groups, others)), dma((groups, others)), dma((groups, chips)), dma((groups, chips)),
+            dma((3, chips)), dma((3, chips)), dma((groups, others)), dma((groups, others)),
             dma((groups,)), dma((groups,)),
-            dma((2, 2, depth)), dma((2, 2, depth)), dma((2, 2 * depth, across)), dma((2, 2 * depth, across)),
+            dma((2, 2, depth - 1)), dma((2, 2, depth - 1)),
+            dma((2, 2 * depth - 1, across - 1)), dma((2, 2 * depth - 1, across - 1)),
             dma((chips,)), dma((chips,)), dma((chips,)), dma((chips,)),
             dma((groups,)), dma((groups,)), dma((groups,)), dma((groups,)), dma((groups, 2)), dma((groups, 2)),
             dma((lanes,)), dma((lanes,)), dma, dma,
@@ -633,6 +662,22 @@
         moe_in, cotangent, routes.T, route_weight.T, norm_mean[None, :], norm_rstd[None, :], conv_pre, ln_gain[None, :], ln_shift[None, :], taps,
         w_gate, w_up, w_down, w_proj,
     )
+    return pl.pallas_call(
+        write_kernel,
+        out_shape=tuple(jax.ShapeDtypeStruct(result.shape, result.dtype) for result in results),
+        in_specs=[inside] * 5,
+        out_specs=(outside,) * 5,
+        scratch_shapes=[dma((5,))],
+        compiler_params=pltpu.CompilerParams(vmem_limit_bytes=16 * 1024 * 1024),
+    )(*results)
+
+
+def write_kernel(*refs):
+    copies = [pltpu.make_async_copy(refs[index], refs[5 + index], refs[10].at[index]) for index in range(5)]
+    for copy in copies:
+        copy.start()
+    for copy in copies:
+        copy.wait()
 
 
 def solution(mesh):

time: 110 us -> 89 us (0.81)
  Pallas kernels: 103 us -> 88 us
  local copies, waits for them, and re-layouts: 5.82 us -> 0 us
    pallas_call x1, Pallas kernels: 103 us -> 84.6 us  [on_device(): pl.pallas_call(functools.partial(layer_kernel, groups, lanes, across), ou...]
    unnamed x5 -> x0, local copies, waits for them, and re-layouts: 5.82 us -> none
    pallas_call x0 -> x1, Pallas kernels: none -> 3.36 us  [on_device(): pl.pallas_call(write_kernel, out_shape=tuple((jax.ShapeDtypeStruct(result...]
where the time goes in v2:
time: 89 us; the launch traced here: 88.8 us
  Pallas kernels  88 us (99%)
    pallas_call x1, Pallas kernels, on_device(): pl.pallas_call(functools.partial(layer_kernel, groups, lanes, across), ou...  84.6 us
    pallas_call x1, Pallas kernels, on_device(): pl.pallas_call(write_kernel, out_shape=tuple((jax.ShapeDtypeStruct(result...  3.36 us

profile of v2, /device:TPU:0, one launch (start us, length us, event | category | flops | bytes accessed | tf_op | source)
XLA Modules:
  0.0 88.8 jit_solution(4588709464910872063)
XLA Ops:
  0.6 84.6 %shard_map.173 = (bf16[1,896,2048]{2,1,0:T(8,128)(2,1)S(1)}, bf16[1,896,2048]{2,1,0:T(8,128)(2,1)S(1)}, bf16[192,512]{1,0:T(8,128)(2,1)S(1)}, f32[256,512]{1,0:T(8,128)S(1)}, bf16[192,512]{1,0:T(8,128)(2,1)S(1)}) custom-call(bf16[192,512]{1,0:T(8,128)(2,1)} %moe_ref.1, bf16[192,512]{1,0:T(8,128)(2,1)} %cot_ref.1, s32[2,192]{1,0:T(2,128)} %bitcast.6, ...), custom_call_target="tpu_custom_call" | custom-call | tf_op jit(solution)/shard_map/pallas_call | solution.py:625
  85.3 3.4 %shard_map.174 = (bf16[1,896,2048]{2,1,0:T(8,128)(2,1)}, bf16[1,896,2048]{2,1,0:T(8,128)(2,1)}, bf16[192,512]{1,0:T(8,128)(2,1)}, f32[256,512]{1,0:T(8,128)}, bf16[192,512]{1,0:T(8,128)(2,1)}) custom-call(bf16[1,896,2048]{2,1,0:T(8,128)(2,1)S(1)} %get-tuple-element.10.refs_0_, bf16[1,896,2048]{2,1,0:T(8,128)(2,1)S(1)} %get-tuple-element.11.refs_1_, ...), custom_call_target="tpu_custom_call" | custom-call | tf_op jit(solution)/shard_map/pallas_call | solution.py:665

commit v3 on v2

--- a/solution.py
+++ b/solution.py
@@ -128,9 +128,10 @@
 
     outgoing = []
 
-    def go(copy):
+    def go(copy, alone=True):
         copy.start()
-        outgoing.append(copy)
+        if alone:
+            outgoing.append(copy)
         return copy
 
     dispatched, crossed, shared = ({}, {}, {})
@@ -138,26 +139,26 @@
     def forward(step):
         for turn in range(1, chips):
             crossed[step, turn] = go(remote(
-                at_slot(step, lane), at_slot(step, lane), dy_s.at[step, turn - 1], dy_r.at[step, turn - 1],
+                at_slot(step, lane), at_slot(step, lane), dy_s.at[turn - 1], dy_r.at[step, turn - 1],
                 (group, flipped(lane, 2 * turn)),
-            ))
+            ), alone=False)
         shared[step, 0] = go(remote(
-            at_slot(step, lane), at_slot(step, lane), dc_s.at[step, 0], dc_r.at[step, 0], partner
-        ))
+            at_slot(step, lane), at_slot(step, lane), dc_s.at[0], dc_r.at[step, 0], partner
+        ), alone=False)
 
     def relay(step):
         for turn in range(1, chips):
             crossed[step, turn].wait_recv()
             peer = flipped(lane, 2 * turn)
             shared[step, turn] = go(remote(
-                at_slot(step, peer), at_slot(step, peer), dc_s.at[step, turn], dc_r.at[step, turn], partner
-            ))
+                at_slot(step, peer), at_slot(step, peer), dc_s.at[turn], dc_r.at[step, turn], partner
+            ), alone=False)
 
     def dispatch(step):
         dispatched[step] = go(remote(
             send.at[:, pl.ds(step * cap, cap)], at_slot(step, lane),
-            dsp_s.at[step], dsp_r.at[step], (flipped(group, step), lane),
-        ))
+            dsp_s.at[0], dsp_r.at[step], (flipped(group, step), lane),
+        ), alone=False)
 
     forward(0)
     for step in range(1, groups // 2):
@@ -324,8 +325,8 @@
                 ).astype(BF)
                 back_across[step, turn] = go(remote(
                     summed.at[turn - 1, pl.ds(step * cap, cap)], arrived.at[turn - 1, pl.ds(step * cap, cap)],
-                    cy_s.at[step, turn - 1], cy_r.at[step, turn - 1], (group, away),
-                ))
+                    cy_s.at[turn - 1], cy_r.at[step, turn - 1], (group, away),
+                ), alone=False)
 
     def send_home(part_index):
         swaps[part_index, 0].wait_recv()
@@ -339,8 +340,8 @@
                 total[here, :] = value.astype(BF)
                 homeward[step] = go(remote(
                     total.at[pl.ds(step * cap, cap)], returned.at[pl.ds(step * cap, cap)],
-                    csp_s.at[step], csp_r.at[step], (flipped(group, step), lane),
-                ))
+                    csp_s.at[0], csp_r.at[step], (flipped(group, step), lane),
+                ), alone=False)
             else:
                 returned[here, :] = value.astype(BF)
 
@@ -416,10 +417,10 @@
     send_home(0)
     activate(2)
     send_home(1)
-    gather_hop(1, 0, True)
     partials(2, nothing)
     chip_sums(2)
     send_home(2)
+    gather_hop(1, 0, True)
 
     span = min(channels, 512)
 
@@ -476,21 +477,21 @@
         owner = flipped(group, step)
         travelling[step] = go(remote(
             mix.at[tile(place_of_four, quarter), piece_of(owner)], pieces.at[step, place_of_four],
-            p_s.at[step], p_r.at[step], (owner, lane),
-        ))
+            p_s.at[0], p_r.at[step], (owner, lane),
+        ), alone=False)
 
     def piece_forward(step):
         travelling[step].wait_recv()
         here = pieces.at[step, place_of_four]
         piece_across[step] = go(remote(
-            here, here, py_s.at[step], py_r.at[step], (group, flipped(lane, 2))
-        ))
-        piece_shared[step, 0] = go(remote(here, here, pc_s.at[step, 0], pc_r.at[step, 0], partner))
+            here, here, py_s.at[0], py_r.at[step], (group, flipped(lane, 2))
+        ), alone=False)
+        piece_shared[step, 0] = go(remote(here, here, pc_s.at[0], pc_r.at[step, 0], partner), alone=False)
 
     def piece_relay(step):
         piece_across[step].wait_recv()
         here = pieces.at[step, flipped(place_of_four, 2)]
-        piece_shared[step, 1] = go(remote(here, here, pc_s.at[step, 1], pc_r.at[step, 1], partner))
+        piece_shared[step, 1] = go(remote(here, here, pc_s.at[1], pc_r.at[step, 1], partner), alone=False)
 
     gather_rest(0)
     whole_proj = gathered[:, 0:proj_rows, :].reshape(groups * proj_rows, width)
@@ -597,6 +598,21 @@
 
     for copy in outgoing:
         copy.wait_send()
+
+    def all_sent(source, sends, recvs):
+        remote(source, source, sends, recvs, partner).wait_send()
+
+    later = pl.ds(cap, slots - cap)
+    all_sent(send.at[:, later], dsp_s.at[0], dsp_r.at[0])
+    all_sent(total.at[later], csp_s.at[0], csp_r.at[0])
+    for turn in range(chips):
+        all_sent(send, dc_s.at[turn], dc_r.at[0, turn])
+        if turn:
+            all_sent(send, dy_s.at[turn - 1], dy_r.at[0, turn - 1])
+            all_sent(total, cy_s.at[turn - 1], cy_r.at[0, turn - 1])
+    every_piece = pieces.at[pl.ds(1, groups - 1), 0]
+    for sends, recvs in ((p_s.at[0], p_r.at[0]), (py_s.at[0], py_r.at[0]), (pc_s.at[0], pc_r.at[0, 0]), (pc_s.at[1], pc_r.at[0, 1])):
+        all_sent(every_piece, sends, recvs)
 
 
 def on_device(
@@ -645,14 +661,14 @@
             vmem((groups, 4, tokens // 4, piece_width), BF),
             vmem((128, (tokens + 127) // 128 * 128), F32), vmem((tokens, width), F32), vmem((tokens, width), F32),
             vmem((16, tokens), F32), vmem((lanes, 16, tokens), F32), vmem((tokens + rim, width), F32),
-            dma((4,)), dma((groups,)), dma((groups,)),
-            dma((groups, others)), dma((groups, others)), dma((groups, chips)), dma((groups, chips)),
-            dma((3, chips)), dma((3, chips)), dma((groups, others)), dma((groups, others)),
-            dma((groups,)), dma((groups,)),
+            dma((4,)), dma((1,)), dma((groups,)),
+            dma((others,)), dma((groups, others)), dma((chips,)), dma((groups, chips)),
+            dma((3, chips)), dma((3, chips)), dma((others,)), dma((groups, others)),
+            dma((1,)), dma((groups,)),
             dma((2, 2, depth - 1)), dma((2, 2, depth - 1)),
             dma((2, 2 * depth - 1, across - 1)), dma((2, 2 * depth - 1, across - 1)),
             dma((chips,)), dma((chips,)), dma((chips,)), dma((chips,)),
-            dma((groups,)), dma((groups,)), dma((groups,)), dma((groups,)), dma((groups, 2)), dma((groups, 2)),
+            dma((1,)), dma((groups,)), dma((1,)), dma((groups,)), dma((2,)), dma((groups, 2)),
             dma((lanes,)), dma((lanes,)), dma, dma,
         ],
         compiler_params=pltpu.CompilerParams(

time: 89 us -> 88.2 us (level)
  no operation moved by 1% of the time
where the time goes in v3:
time: 88.2 us; the launch traced here: 88.1 us
  Pallas kernels  87.3 us (99%)
    pallas_call x1, Pallas kernels, on_device(): pl.pallas_call(functools.partial(layer_kernel, groups, lanes, across), ou...  83.9 us
    pallas_call x1, Pallas kernels, on_device(): pl.pallas_call(write_kernel, out_shape=tuple((jax.ShapeDtypeStruct(result...  3.36 us

profile of v3, /device:TPU:0, one launch (start us, length us, event | category | flops | bytes accessed | tf_op | source)
XLA Modules:
  0.0 88.1 jit_solution(7071277131991212630)
XLA Ops:
  0.6 83.9 %shard_map.173 = (bf16[1,896,2048]{2,1,0:T(8,128)(2,1)S(1)}, bf16[1,896,2048]{2,1,0:T(8,128)(2,1)S(1)}, bf16[192,512]{1,0:T(8,128)(2,1)S(1)}, f32[256,512]{1,0:T(8,128)S(1)}, bf16[192,512]{1,0:T(8,128)(2,1)S(1)}) custom-call(bf16[192,512]{1,0:T(8,128)(2,1)} %moe_ref.1, bf16[192,512]{1,0:T(8,128)(2,1)} %cot_ref.1, s32[2,192]{1,0:T(2,128)} %bitcast.6, ...), custom_call_target="tpu_custom_call" | custom-call | tf_op jit(solution)/shard_map/pallas_call | solution.py:641
  84.6 3.4 %shard_map.174 = (bf16[1,896,2048]{2,1,0:T(8,128)(2,1)}, bf16[1,896,2048]{2,1,0:T(8,128)(2,1)}, bf16[192,512]{1,0:T(8,128)(2,1)}, f32[256,512]{1,0:T(8,128)}, bf16[192,512]{1,0:T(8,128)(2,1)}) custom-call(bf16[1,896,2048]{2,1,0:T(8,128)(2,1)S(1)} %get-tuple-element.10.refs_0_, bf16[1,896,2048]{2,1,0:T(8,128)(2,1)S(1)} %get-tuple-element.11.refs_1_, ...), custom_call_target="tpu_custom_call" | custom-call | tf_op jit(solution)/shard_map/pallas_call | solution.py:681
